TPU v7x, 32 devices: a whole 2x2x4 slice. The times are simulated.
32 devices in a mesh: grp: 2 (over y), sp: 4 (over z), tp: 4 (over x, core).
Axes of the slice: x: 2, y: 2, z: 4, core: 2. Of those that a mesh axis runs over, the one named last changes fastest.
Arguments:
- latents: bfloat16 [4096, 2048], P(('grp', 'sp', 'tp')), parts along dimension 0, may hold values from -6 to 6
- conv_value: bfloat16 [4096, 1024], P(('grp', 'sp'), 'tp'), parts along dimension 0, may hold values from -6 to 6
- conv_gate: bfloat16 [4096, 1024], P(('grp', 'sp'), 'tp'), parts along dimension 0, may hold values from -6 to 6
- conv_taps: float32 [31, 1024], P(None, 'tp'), may hold values from -2.2 to 2.2
- conv_gain: float32 [1024], P('tp'), may hold values from 0.1 to 1.9
- point_weight: bfloat16 [1024, 2048], P('tp'), may hold values from -0.1875 to 0.1875
- channel_gain: float32 [2048], replicated, may hold values from 0.1 to 1.9
- expert_ids: int32 [4096, 2], P(('grp', 'sp', 'tp')), parts along dimension 0, may hold values from 0 to 15, all different within a row; in each aligned block of 128 rows (0 to 127, 128 to 255, ...) at most 32 rows name the same one
- expert_weights: float32 [4096, 2], P(('grp', 'sp', 'tp')), parts along dimension 0, may hold values from 0.2 to 1
- gate_weight: bfloat16 [16, 2048, 768], P(('sp', 'tp')), may hold values from -0.125 to 0.125
- up_weight: bfloat16 [16, 2048, 768], P(('sp', 'tp')), may hold values from -0.125 to 0.125
- down_weight: bfloat16 [16, 768, 2048], P(('sp', 'tp')), may hold values from -0.21875 to 0.21875
Outputs:
- result: bfloat16 [4096, 2048], P(('grp', 'sp', 'tp')), parts along dimension 0
There are 2 independent parts, one for each index of `grp`. A program takes and returns all parts, laid end to end along the dimension named above; an argument that names none is the same for every part. Nothing has to cross between parts.
Inputs may be any that keep to these rules, and one draw needn't show every extreme that they name: `expert_ids`: each row names 2 different experts. Within the rows of one device (aligned blocks of 128 rows) no expert is named by more than 32 rows, and in some device's rows some expert is named by exactly 32.
All inputs are finite; a program needn't handle non-finite values.
Results may differ from a plain program's by a relative error of at most 0.012.
Values may be sent and summed in bfloat16 or wider, within the bound.
A program may use at most 64 MiB of HBM per device.

v0:
```python
import jax
import jax.numpy as jnp
from jax import lax
from jax.sharding import PartitionSpec as P


def with_halo(block, sides, width):
    for axis, dim in sides:
        count = lax.axis_size(axis)
        forward = [(i, i + 1) for i in range(count - 1)]
        backward = [(target, source) for source, target in forward]
        low = lax.ppermute(
            lax.slice_in_dim(block, block.shape[dim] - width, None, axis=dim), axis, forward
        )
        high = lax.ppermute(lax.slice_in_dim(block, 0, width, axis=dim), axis, backward)
        block = jnp.concatenate([low, block, high], axis=dim)
    return block


def shards(
    latents,
    conv_value,
    conv_gate,
    conv_taps,
    conv_gain,
    point_weight,
    channel_gain,
    expert_ids,
    expert_weights,
    gate_weight,
    up_weight,
    down_weight,
):
    gated_value = (
        conv_value.astype(jnp.float32) * jax.nn.sigmoid(conv_gate.astype(jnp.float32))
    ).astype(jnp.bfloat16)
    tap_count = conv_taps.shape[0]
    half_span = tap_count // 2
    block_rows = gated_value.shape[0]
    padded = with_halo(gated_value, (("sp", 0),), half_span).astype(jnp.float32)
    mixed_rows = jnp.zeros(gated_value.shape, jnp.float32)
    for offset in range(tap_count):
        mixed_rows = mixed_rows + conv_taps[offset][None, :] * padded[offset : offset + block_rows]
    width_all = conv_value.shape[1] * lax.axis_size("tp")
    sum_values, squares = lax.psum(
        (jnp.sum(mixed_rows, axis=1), jnp.sum(mixed_rows * mixed_rows, axis=1)), "tp"
    )
    center = (sum_values / width_all)[:, None]
    spread = (squares / width_all)[:, None] - center * center
    activated = jax.nn.silu((mixed_rows - center) * lax.rsqrt(spread + 0.05) * conv_gain).astype(
        jnp.bfloat16
    )
    row_count = latents.shape[0]
    by_token = lax.all_to_all(activated, "tp", split_axis=0, concat_axis=1, tiled=True)
    branch = jnp.dot(
        by_token,
        lax.all_gather(point_weight, "tp", axis=0, tiled=True),
        preferred_element_type=jnp.float32,
    )
    after_wide = (latents.astype(jnp.float32) + branch).astype(jnp.bfloat16).astype(jnp.float32)
    scale_rows = lax.rsqrt(jnp.mean(after_wide * after_wide, axis=1, keepdims=True) + 0.01)
    expert_in = (after_wide * scale_rows * channel_gain).astype(jnp.bfloat16)
    local_count = gate_weight.shape[0]
    members = lax.axis_size(("sp", "tp"))
    experts = local_count * members
    top_count = expert_ids.shape[1]
    capacity = 2 * top_count * row_count // experts
    feature_count = expert_in.shape[1]
    flat_ids = expert_ids.reshape(-1)
    onehot = (flat_ids[:, None] == jnp.arange(experts, dtype=jnp.int32)[None, :]).astype(jnp.int32)
    earlier = jnp.sum((jnp.cumsum(onehot, axis=0) - onehot) * onehot, axis=1)
    target = flat_ids * capacity + earlier
    source_rows = jnp.repeat(expert_in, top_count, axis=0)
    outbox = (
        jnp.zeros((experts * capacity, feature_count), jnp.bfloat16).at[target].set(source_rows)
    )
    outbox = outbox.reshape(experts, capacity, feature_count)
    arrived = lax.all_to_all(outbox, ("sp", "tp"), split_axis=0, concat_axis=0, tiled=True)
    slot_count = arrived.shape[1]
    grouped = arrived.reshape(members, local_count, slot_count, feature_count)
    gate_part = jnp.einsum(
        "secd,edf->secf", grouped, gate_weight, preferred_element_type=jnp.float32
    )
    up_part = jnp.einsum("secd,edf->secf", grouped, up_weight, preferred_element_type=jnp.float32)
    hidden = (jax.nn.silu(gate_part) * up_part).astype(jnp.bfloat16)
    answer = jnp.einsum(
        "secf,efd->secd", hidden, down_weight, preferred_element_type=jnp.float32
    ).astype(jnp.bfloat16)
    answer = answer.reshape(members * local_count, slot_count, feature_count)
    returned = lax.all_to_all(answer, ("sp", "tp"), split_axis=0, concat_axis=0, tiled=True)
    picked = returned.reshape(experts * capacity, feature_count)[target].astype(jnp.float32)
    picked = picked.reshape(row_count, top_count, feature_count)
    routed = jnp.sum(expert_weights[:, :, None] * picked, axis=1)
    return (after_wide + routed).astype(jnp.bfloat16)


def solution(mesh):
    return jax.shard_map(
        shards,
        mesh=mesh,
        in_specs=(
            P(("grp", "sp", "tp"), None),
            P(("grp", "sp"), "tp"),
            P(("grp", "sp"), "tp"),
            P(None, "tp"),
            P("tp"),
            P("tp", None),
            P(),
            P(("grp", "sp", "tp"), None),
            P(("grp", "sp", "tp"), None),
            P(("sp", "tp"), None, None),
            P(("sp", "tp"), None, None),
            P(("sp", "tp"), None, None),
        ),
        out_specs=P(("grp", "sp", "tp"), None),
        check_vma=False,
    )
```

profile of v0, /device:TPU:11, one launch (start us, length us, event | category | flops | bytes accessed | tf_op | source)
XLA Modules:
  0.0 199.7 jit_solution(13373950620552734918)
XLA Ops:
  7.3 1.3 multiply_convert_fusion.2
  8.6 3.2 %collective-permute-start = (bf16[15,256]{1,0:T(8,128)(2,1)S(1)}, bf16[15,256]{1,0:T(8,128)(2,1)S(1)}, u32[]{:S(2)}, u32[]{:S(2)}) collective-permute-start(bf16[15,256]{1,0:T(8,128)(2,1)S(1)} %get-tuple-element.10), channel_id=1, source_target_pairs={{0,4},{4,8},{8,12},{1,5},{5,9},{9,13},{2,6},{6,10},{10,14},{3,7},{... | collective-permute-start | bytes 23048 | tf_op jit(solution)/shard_map/ppermute | solution.py:12
  11.8 2.1 %collective-permute-start.1 = (bf16[15,256]{1,0:T(8,128)(2,1)S(1)}, bf16[15,256]{1,0:T(8,128)(2,1)S(1)}, u32[]{:S(2)}, u32[]{:S(2)}) collective-permute-start(bf16[15,256]{1,0:T(8,128)(2,1)S(1)} %get-tuple-element.11), channel_id=1, source_target_pairs={{4,0},{8,4},{12,8},{5,1},{9,5},{13,9},{6,2},{10,6},{14,10},{7,3},{... | collective-permute-start | bytes 23048 | tf_op jit(solution)/shard_map/ppermute | solution.py:15
  20.0 3.8 %fusion.59 = (f32[512]{0:T(512)S(1)}, f32[512]{0:T(512)S(1)}, f32[512,256]{1,0:T(8,128)}) fusion(f32[542,256]{1,0:T(8,128)S(1)} %maximum_convert_fusion, f32[256]{0:T(256)} %bitcast.132, f32[256]{0:T(256)} %bitcast.133, f32[256]{0:T(256)} %bitcast.135, f32[256]{0:T(256)} %bitcast.136, f32[256]{0:T(256)} %bitcast.137, f32[256]{0:T(256)} %bitcast.138, ...), kind=kLoop, calls=%fused_computation.107 | loop fusion | flops 8387584 | bytes 16813056 | tf_op jit(solution)/shard_map/reduce_sum | solution.py:46
  23.8 6.5 %all-reduce = (f32[512]{0:T(512)S(1)}, f32[512]{0:T(512)S(1)}) all-reduce(f32[512]{0:T(512)S(1)} %get-tuple-element.6, f32[512]{0:T(512)S(1)} %get-tuple-element.5), channel_id=1, replica_groups=mesh['grp'=2,'sp'=4,'tp'=4] {'tp'}, use_global_device_ids=true, to_apply=%region_3.0 | all-reduce | flops 1024 | bytes 8192 | tf_op jit(solution)/shard_map/psum | solution.py:45
  30.3 2.0 multiply_convert_fusion.1
  32.3 5.1 %all-to-all-start = ((bf16[4,128,256]{2,1,0:T(8,128)(2,1)}), bf16[4,128,256]{2,1,0:T(8,128)(2,1)S(1)}, u32[]{:S(2)}, u32[]{:S(2)}) async-start(bf16[4,128,256]{2,1,0:T(8,128)(2,1)} %bitcast.121), calls=%async_computation | async-start | bytes 524288 | tf_op jit(solution)/shard_map/all_to_all | solution.py:54
  37.4 7.4 %all-to-all-done = bf16[4,128,256]{2,1,0:T(8,128)(2,1)S(1)} async-done(((bf16[4,128,256]{2,1,0:T(8,128)(2,1)}), bf16[4,128,256]{2,1,0:T(8,128)(2,1)S(1)}, u32[]{:S(2)}, u32[]{:S(2)}) %all-to-all-start) | async-done | bytes 262176 | tf_op jit(solution)/shard_map/all_to_all | solution.py:54
  45.5 1.1 copy.19
  47.0 3.1 %multiply_reduce_fusion.1 = (f32[128]{0:T(128)S(1)}, f32[128,2048]{1,0:T(8,128)S(1)}) fusion(bf16[128,1024]{0,1:T(8,128)(2,1)S(1)} %bitcast.119, bf16[1024,2048]{1,0:T(8,128)(2,1)} %all-gather.2.cloned.1.call-done, bf16[128,2048]{1,0:T(8,128)(2,1)} %param.12), kind=kOutput, calls=%fused_computation.23 | convolution fusion | flops 538443648 | bytes 6029824 | tf_op jit(solution)/shard_map/dot_general | solution.py:55
  50.1 1.0 copy-done.1
  51.3 1.6 broadcast_in_dim.5
  52.9 2.3 %reshape.122 = bf16[256,2048]{1,0:T(8,128)(2,1)} reshape(bf16[128,2,2048]{2,1,0:T(2,128)(2,1)} %broadcast_in_dim.5) | data formatting | bytes 2097152 | tf_op jit(solution)/shard_map/reshape | solution.py:73
  55.1 4.4 %scatter_custom_fusion = bf16[512,2048]{1,0:T(8,128)(2,1)} fusion(s32[256]{0:T(256)S(1)} %bitcast.154, bf16[256,2048]{1,0:T(8,128)(2,1)} %reshape.122, bf16[]{:T(256)} %constant.9.clone.1), kind=kCustom, calls=%fused_computation.24 | custom fusion | bytes 2097664 | tf_op jit(solution)/shard_map/scatter | solution.py:75
  59.6 53.6 %all_to_all.29 = bf16[16,32,2048]{2,1,0:T(8,128)(2,1)S(1)} all-to-all(bf16[16,32,2048]{2,1,0:T(8,128)(2,1)} %bitcast.118), channel_id=1, replica_groups=mesh['grp'=2,'sp'=4,'tp'=4] {'sp','tp'}, dimensions={0} | all-to-all | bytes 4194304 | tf_op jit(solution)/shard_map/all_to_all | solution.py:78
  113.2 1.3 copy-done.3
  114.5 3.0 %fusion.4 = f32[16,32,768]{2,1,0:T(8,128)} fusion(bf16[16,32,2048]{2,1,0:T(8,128)(2,1)S(1)} %all_to_all.29, bf16[1,2048,768]{2,1,0:T(8,128)(2,1)S(1)} %copy-done.10), kind=kOutput, calls=%fused_computation.6 | convolution fusion | flops 1610612736 | bytes 6815744 | tf_op jit(solution)/shard_map/secd,edf->secf/dot_general | solution.py:81
  117.5 8.3 %fusion.6 = bf16[16,32,2048]{2,1,0:T(8,128)(2,1)} fusion(bf16[1,768,2048]{2,1,0:T(8,128)(2,1)S(1)} %copy-done, bf16[16,32,2048]{2,1,0:T(8,128)(2,1)} %copy-done.3, bf16[1,2048,768]{2,1,0:T(8,128)(2,1)} %param.22, f32[16,32,768]{2,1,0:T(8,128)} %fusion.4), kind=kOutput, calls=%fused_computation.8 | convolution fusion | flops 3224633344 | bytes 12058624 | tf_op jit(solution)/shard_map/secf,efd->secd/dot_general | solution.py:86
  125.7 5.2 %all-to-all-start.2 = ((bf16[16,32,2048]{2,1,0:T(8,128)(2,1)}), bf16[16,32,2048]{2,1,0:T(8,128)(2,1)}, u32[]{:S(2)}, u32[]{:S(2)}) async-start(bf16[16,32,2048]{2,1,0:T(8,128)(2,1)} %fusion.6), calls=%async_computation.2 | async-start | bytes 4194304 | tf_op jit(solution)/shard_map/all_to_all | solution.py:90
  131.0 47.4 %all-to-all-done.2 = bf16[16,32,2048]{2,1,0:T(8,128)(2,1)} async-done(((bf16[16,32,2048]{2,1,0:T(8,128)(2,1)}), bf16[16,32,2048]{2,1,0:T(8,128)(2,1)}, u32[]{:S(2)}, u32[]{:S(2)}) %all-to-all-start.2) | async-done | bytes 2097184 | tf_op jit(solution)/shard_map/all_to_all | solution.py:90
  178.4 5.2 %gather_fusion = bf16[256,2048]{1,0:T(8,128)(2,1)} fusion(bf16[512,2048]{1,0:T(8,128)(2,1)} %bitcast.53, s32[1024]{0:T(1024)S(1)} %pad_clamp_fusion), kind=kCustom, calls=%fused_computation | custom fusion | bytes 2098176 | tf_op jit(solution)/shard_map/gather | solution.py:91
  183.6 3.4 %reshape.109 = f32[128,2,2048]{2,1,0:T(2,128)} reshape(bf16[256,2048]{1,0:T(8,128)(2,1)} %gather_fusion) | data formatting | bytes 3145728 | tf_op jit(solution)/shard_map/convert_element_type | solution.py:91
  187.0 4.9 %multiply_reduce_fusion = f32[128,2048]{1,0:T(8,128)S(1)} fusion(f32[128,2,2048]{2,1,0:T(2,128)} %reshape.109, f32[128,2]{1,0:T(8,128)S(1)} %copy.20), kind=kLoop, calls=%fused_computation.12 | loop fusion | flops 786432 | bytes 3146752 | tf_op jit(solution)/shard_map/reduce_sum | solution.py:93
  191.9 0.9 add_convert_fusion
  (47 shorter events, 8.1 us)
Async XLA Ops:
  6.5 110.9 %copy-start = (bf16[1,768,2048]{2,1,0:T(8,128)(2,1)S(1)}, bf16[1,768,2048]{2,1,0:T(8,128)(2,1)}, u32[]{:S(2)}) copy-start(bf16[1,768,2048]{2,1,0:T(8,128)(2,1)} %param.23) | copy-start | bytes 9437188
  6.5 9.8 %copy-start.7 = (s32[128,2]{0,1:T(2,128)S(1)}, s32[128,2]{0,1:T(2,128)}, u32[]{:S(2)}) copy-start(s32[128,2]{0,1:T(2,128)} %param.19) | copy-start | bytes 3076
  6.5 10.4 %copy-start.5 = (f32[31,256]{1,0:T(8,128)S(1)}, f32[31,256]{1,0:T(8,128)}, u32[]{:S(2)}) copy-start(f32[31,256]{1,0:T(8,128)} %param.15) | copy-start | bytes 95236
  6.5 40.4 %all-gather.2.cloned.1.call-start = ((), (), s32[]{:S(2)}) async-start(), calls=%async_computation.3 | async-start | bytes 5242880 | tf_op jit(solution)/shard_map/all_gather | solution.py:57
  8.6 11.3 %collective-permute-start = (bf16[15,256]{1,0:T(8,128)(2,1)S(1)}, bf16[15,256]{1,0:T(8,128)(2,1)S(1)}, u32[]{:S(2)}, u32[]{:S(2)}) collective-permute-start(bf16[15,256]{1,0:T(8,128)(2,1)S(1)} %get-tuple-element.10), channel_id=1, source_target_pairs={{0,4},{4,8},{8,12},{1,5},{5,9},{9,13},{2,6},{6,10},{10,14},{3,7},{... | collective-permute-start | bytes 23048 | tf_op jit(solution)/shard_map/ppermute | solution.py:12
  11.8 8.1 %collective-permute-start.1 = (bf16[15,256]{1,0:T(8,128)(2,1)S(1)}, bf16[15,256]{1,0:T(8,128)(2,1)S(1)}, u32[]{:S(2)}, u32[]{:S(2)}) collective-permute-start(bf16[15,256]{1,0:T(8,128)(2,1)S(1)} %get-tuple-element.11), channel_id=1, source_target_pairs={{4,0},{8,4},{12,8},{5,1},{9,5},{13,9},{6,2},{10,6},{14,10},{7,3},{... | collective-permute-start | bytes 23048 | tf_op jit(solution)/shard_map/ppermute | solution.py:15
  19.9 10.3 %copy-start.8 = (f32[256]{0:T(256)S(1)}, f32[256]{0:T(256)}, u32[]{:S(2)}) copy-start(f32[256]{0:T(256)} %param.16) | copy-start | bytes 3076
  32.3 12.5 %all-to-all-start = ((bf16[4,128,256]{2,1,0:T(8,128)(2,1)}), bf16[4,128,256]{2,1,0:T(8,128)(2,1)S(1)}, u32[]{:S(2)}, u32[]{:S(2)}) async-start(bf16[4,128,256]{2,1,0:T(8,128)(2,1)} %bitcast.121), calls=%async_computation | async-start | bytes 524288 | tf_op jit(solution)/shard_map/all_to_all | solution.py:54
  44.8 0.7 copy-start.4
  47.0 4.1 %copy-start.6 = (f32[2048]{0:T(1024)S(1)}, f32[2048]{0:T(1024)}, u32[]{:S(2)}) copy-start(f32[2048]{0:T(1024)} %param.18) | copy-start | bytes 24580
  50.1 1.0 copy-start.1
  59.6 54.9 %copy-start.10 = (bf16[1,2048,768]{2,1,0:T(8,128)(2,1)S(1)}, bf16[1,2048,768]{2,1,0:T(8,128)(2,1)}, u32[]{:S(2)}) copy-start(bf16[1,2048,768]{2,1,0:T(8,128)(2,1)} %param.21) | copy-start | bytes 9437188
  113.2 1.3 copy-start.3
  125.7 5.2 %copy-start.9 = (f32[128,2]{0,1:T(2,128)S(1)}, f32[128,2]{0,1:T(2,128)}, u32[]{:S(2)}) copy-start(f32[128,2]{0,1:T(2,128)} %param.20) | copy-start | bytes 3076
  125.7 52.7 %all-to-all-start.2 = ((bf16[16,32,2048]{2,1,0:T(8,128)(2,1)}), bf16[16,32,2048]{2,1,0:T(8,128)(2,1)}, u32[]{:S(2)}, u32[]{:S(2)}) async-start(bf16[16,32,2048]{2,1,0:T(8,128)(2,1)} %fusion.6), calls=%async_computation.2 | async-start | bytes 4194304 | tf_op jit(solution)/shard_map/all_to_all | solution.py:90
  187.0 4.9 %copy-start.2 = (f32[128,2048]{1,0:T(8,128)S(1)}, f32[128,2048]{1,0:T(8,128)}, u32[]{:S(2)}) copy-start(f32[128,2048]{1,0:T(8,128)} %copy-done.1) | copy-start | bytes 3145732
Sparse Core Ops, SparseCore 0:
  8.9 38.0 all-gather.1
where the time goes:
time: 200 us
  blocking collectives  60.1 us (30%)
  waiting for transfers between devices  55.9 us (28%)
  local copies, waits for them, and re-layouts  25.2 us (13%)
  starting transfers between devices  15.6 us (8%)
  other arithmetic  15.1 us (8%)
  matrix products  14.4 us (7%)
  between operations  13.5 us (7%)
    all_to_all x1, blocking collectives, shards(): lax.all_to_all(outbox, ('sp', 'tp'), split_axis=0, concat_axis=0, tiled=T...  53.6 us
    all_to_all x1, waiting for transfers between devices, shards(): lax.all_to_all(answer, ('sp', 'tp'), split_axis=0, concat_axis=0, tiled=T...  47.4 us
    dot_general x1, matrix products, shards(): jnp.einsum('secf,efd->secd', hidden, down_weight, preferred_element_type=...  8.28 us
    all_to_all x1, waiting for transfers between devices, shards(): lax.all_to_all(activated, 'tp', split_axis=0, concat_axis=1, tiled=True)  7.37 us
    psum x1, blocking collectives, shards(): lax.psum((jnp.sum(mixed_rows, axis=1), jnp.sum(mixed_rows * mixed_rows, a...  6.47 us
    gather x1, local copies, waits for them, and re-layouts, shards(): returned.reshape(experts * capacity, feature_count)[target]  5.2 us
    all_to_all x1, starting transfers between devices, shards(): lax.all_to_all(answer, ('sp', 'tp'), split_axis=0, concat_axis=0, tiled=T...  5.16 us
    all_to_all x1, starting transfers between devices, shards(): lax.all_to_all(activated, 'tp', split_axis=0, concat_axis=1, tiled=True)  5.12 us
  transfers between devices with their start and end apart: 5, of which 3 were waited for; matrix products, arithmetic and copies ran while one was open for 7% of the time, Pallas kernels for 0%

commit v1 on v0

--- a/solution.py
+++ b/solution.py
@@ -1,6 +1,10 @@
+import functools
+
 import jax
 import jax.numpy as jnp
 from jax import lax
+from jax.experimental import pallas as pl
+from jax.experimental.pallas import tpu as pltpu
 from jax.sharding import PartitionSpec as P
 
 
@@ -15,6 +19,327 @@
         high = lax.ppermute(lax.slice_in_dim(block, 0, width, axis=dim), axis, backward)
         block = jnp.concatenate([low, block, high], axis=dim)
     return block
+
+
+MESH = pl.DeviceIdType.MESH
+CHUNKS = 4
+
+
+def expert_kernel(
+    n, tp, cap, x_hbm, tab_hbm, after_ref, wg_hbm, wu_hbm, wd_hbm, out_ref,
+    toks, tabs, comp, arr, back, inc, acc, wg, wu, wd, hid,
+    own_sem, w_sem, tok_send, tok_recv, tab_send, tab_recv,
+    piece_send, piece_recv, back_send, back_recv, sum_send, sum_recv,
+):
+    z = lax.axis_index("sp")
+    t = lax.axis_index("tp")
+    rows, width = after_ref.shape
+    slots = tp * cap
+    hidden_width = wg.shape[1]
+    part_rows = rows // CHUNKS
+    own_tok = pltpu.make_async_copy(x_hbm, toks.at[z], own_sem.at[0])
+    own_tab = pltpu.make_async_copy(tab_hbm, tabs.at[z], own_sem.at[1])
+    own_tok.start()
+    own_tab.start()
+    loads = [
+        pltpu.make_async_copy(a, b, w_sem.at[i])
+        for i, (a, b) in enumerate(((wg_hbm.at[0], wg), (wu_hbm.at[0], wu), (wd_hbm.at[0], wd)))
+    ]
+    for load in loads:
+        load.start()
+
+    barrier = pltpu.get_barrier_semaphore()
+    for p in range(1, tp):
+        pl.semaphore_signal(
+            barrier, inc=1, device_id={"tp": lax.rem(t + p, tp)}, device_id_type=MESH
+        )
+
+    @pl.when(z > 0)
+    def _():
+        pl.semaphore_signal(barrier, inc=1, device_id={"sp": z - 1}, device_id_type=MESH)
+
+    @pl.when(z < n - 1)
+    def _():
+        pl.semaphore_signal(barrier, inc=1, device_id={"sp": z + 1}, device_id_type=MESH)
+
+    peers = tp - 1 + (z > 0).astype(jnp.int32) + (z < n - 1).astype(jnp.int32)
+    pl.semaphore_wait(barrier, peers)
+
+    own_tok.wait()
+    own_tab.wait()
+
+    def source(j):
+        low = jnp.minimum(z, n - 1 - z)
+        near = jnp.where(j % 2 == 1, z - (j + 1) // 2, z + j // 2)
+        far = jnp.where(z > n - 1 - z, z - (j - low), z + (j - low))
+        return jnp.where(j <= 2 * low, near, far)
+
+    def token_copies(zs, side):
+        target = z + 1 if side else z - 1
+        return [
+            pltpu.make_async_remote_copy(
+                src_ref=ref.at[zs],
+                dst_ref=ref.at[zs],
+                send_sem=ss.at[side, zs],
+                recv_sem=rs.at[zs],
+                device_id={"sp": target},
+                device_id_type=MESH,
+            )
+            for ref, ss, rs in ((tabs, tab_send, tab_recv), (toks, tok_send, tok_recv))
+        ]
+
+    def span(index):
+        return pl.ds(pl.multiple_of(index * cap, 16), cap)
+
+    def exchange(j, to_ref, zs, ss, rs):
+        page = lax.rem(j, 2)
+        for p in range(1, tp):
+            other = lax.rem(t + p, tp)
+            pltpu.make_async_remote_copy(
+                src_ref=comp.at[page, span(other)],
+                dst_ref=to_ref.at[zs, span(t)],
+                send_sem=ss.at[zs],
+                recv_sem=rs.at[zs],
+                device_id={"tp": other},
+                device_id_type=MESH,
+            ).start()
+        to_ref[zs, span(t)] = comp[page, span(t)]
+
+    def wait_pieces(ref, zs, ss, rs):
+        part = ref.at[zs, pl.ds(0, (tp - 1) * cap)]
+        pltpu.make_async_copy(part, part, rs.at[zs]).wait()
+        pltpu.make_async_copy(part, part, ss.at[zs]).wait()
+
+    def sum_copy(zs, k, side):
+        target = z + 1 if side else z - 1
+        slot = jnp.where(target == zs, n, zs) if side else zs
+        piece = pl.ds(k * part_rows, part_rows)
+        return pltpu.make_async_remote_copy(
+            src_ref=toks.at[zs, piece],
+            dst_ref=inc.at[slot, piece],
+            send_sem=sum_send.at[zs, k],
+            recv_sem=sum_recv.at[slot, k],
+            device_id={"sp": target},
+            device_id_type=MESH,
+        )
+
+    def names(zs):
+        table = tabs[zs]
+        base = (z * slots).astype(jnp.float32)
+        place = lax.broadcasted_iota(jnp.int32, (slots, rows), 0).astype(jnp.float32) + base
+        return place == table[0:1, :], place == table[1:2, :], table
+
+    def take(j):
+        zs = source(j)
+
+        @pl.when(j > 0)
+        def _():
+            pltpu.make_async_copy(tabs.at[zs], tabs.at[zs], tab_recv.at[zs]).wait()
+            pltpu.make_async_copy(toks.at[zs], toks.at[zs], tok_recv.at[zs]).wait()
+
+        @pl.when((zs <= z) & (z < n - 1))
+        def _():
+            for copy in token_copies(zs, 1):
+                copy.start()
+
+        @pl.when((zs >= z) & (z > 0))
+        def _():
+            for copy in token_copies(zs, 0):
+                copy.start()
+
+        first, second, _ = names(zs)
+        pick = jnp.where(first | second, 1.0, 0.0).astype(jnp.bfloat16)
+        comp[lax.rem(j, 2)] = jnp.dot(pick, toks[zs], preferred_element_type=jnp.float32).astype(jnp.bfloat16)
+        exchange(j, arr, zs, piece_send, piece_recv)
+
+    def run(j):
+        zs = source(j)
+
+        @pl.when(j == 0)
+        def _():
+            for load in loads:
+                load.wait()
+
+        wait_pieces(arr, zs, piece_send, piece_recv)
+        step = 256
+        for f in range(0, hidden_width, step):
+            gate = jnp.dot(arr[zs], wg[:, f : f + step], preferred_element_type=jnp.float32)
+            up = jnp.dot(arr[zs], wu[:, f : f + step], preferred_element_type=jnp.float32)
+            hid[:, f : f + step] = (jax.nn.silu(gate) * up).astype(jnp.bfloat16)
+        step = 512
+        for c in range(0, width, step):
+            comp[lax.rem(j, 2), :, c : c + step] = jnp.dot(
+                hid[...], wd[:, c : c + step], preferred_element_type=jnp.float32
+            ).astype(jnp.bfloat16)
+        exchange(j, back, zs, back_send, back_recv)
+
+    def merge(j):
+        zs = source(j)
+        wait_pieces(back, zs, back_send, back_recv)
+        first, second, table = names(zs)
+        share = jnp.where(first, table[2:3, :], 0.0) + jnp.where(second, table[3:4, :], 0.0)
+        share = share.T
+        high = share.astype(jnp.bfloat16)
+        rest = (share - high.astype(jnp.float32)).astype(jnp.bfloat16)
+
+        def total():
+            return jnp.dot(high, back[zs], preferred_element_type=jnp.float32) + jnp.dot(
+                rest, back[zs], preferred_element_type=jnp.float32
+            )
+
+        @pl.when((zs <= z) & (z < n - 1))
+        def _():
+            for copy in token_copies(zs, 1):
+                copy.wait_send()
+
+        @pl.when((zs >= z) & (z > 0))
+        def _():
+            for copy in token_copies(zs, 0):
+                copy.wait_send()
+
+        value = total()
+
+        @pl.when(zs == z)
+        def _():
+            acc[...] = value
+
+        @pl.when(zs != z)
+        def _():
+            toks[zs] = value.astype(jnp.bfloat16)
+
+        @pl.when((zs < z) & (z == n - 1))
+        def _():
+            for k in range(CHUNKS):
+                sum_copy(zs, k, 0).start()
+
+        @pl.when((zs > z) & (z == 0))
+        def _():
+            for k in range(CHUNKS):
+                sum_copy(zs, k, 1).start()
+
+    def body(j, carry):
+        @pl.when(j > 0)
+        def _():
+            run(j - 1)
+
+        @pl.when(j < n)
+        def _():
+            take(j)
+
+        @pl.when(j > 0)
+        def _():
+            merge(j - 1)
+
+        return carry
+
+    lax.fori_loop(0, n + 1, body, 0)
+
+    def relay(side):
+        def one(d, carry):
+            zs = z + d if side else z - d
+
+            @pl.when((zs <= n - 1) if side else (zs >= 0))
+            def _():
+                for k in range(CHUNKS):
+                    piece = pl.ds(k * part_rows, part_rows)
+                    spot = inc.at[zs, piece]
+                    pltpu.make_async_copy(spot, spot, sum_recv.at[zs, k]).wait()
+                    toks[zs, piece] = (
+                        toks[zs, piece].astype(jnp.float32) + inc[zs, piece].astype(jnp.float32)
+                    ).astype(jnp.bfloat16)
+                    sum_copy(zs, k, side).start()
+
+            return carry
+
+        lax.fori_loop(1, n - 1, one, 0)
+
+    upper = z > n - 1 - z
+
+    @pl.when(upper & (z < n - 1))
+    def _():
+        relay(0)
+
+    @pl.when(z > 0)
+    def _():
+        relay(1)
+
+    @pl.when((z <= n - 1 - z) & (z < n - 1))
+    def _():
+        relay(0)
+
+    for k in range(CHUNKS):
+        piece = pl.ds(k * part_rows, part_rows)
+
+        @pl.when(z < n - 1)
+        def _():
+            spot = inc.at[z, piece]
+            pltpu.make_async_copy(spot, spot, sum_recv.at[z, k]).wait()
+            acc[piece] = acc[piece] + inc[z, piece].astype(jnp.float32)
+
+        @pl.when(z > 0)
+        def _():
+            spot = inc.at[n, piece]
+            pltpu.make_async_copy(spot, spot, sum_recv.at[n, k]).wait()
+            acc[piece] = acc[piece] + inc[n, piece].astype(jnp.float32)
+
+        out_ref[piece] = (after_ref[piece].astype(jnp.float32) + acc[piece]).astype(jnp.bfloat16)
+
+    def drain(zs, carry):
+        @pl.when(zs != z)
+        def _():
+            for k in range(CHUNKS):
+                spot = toks.at[zs, pl.ds(k * part_rows, part_rows)]
+                pltpu.make_async_copy(spot, spot, sum_send.at[zs, k]).wait()
+
+        return carry
+
+    lax.fori_loop(0, n, drain, 0)
+
+
+def experts_and_back(expert_in, table, after, gate_weight, up_weight, down_weight, cap):
+    n, tp = lax.axis_size("sp"), lax.axis_size("tp")
+    rows, width = expert_in.shape
+    hidden_width = gate_weight.shape[2]
+    slots = tp * cap
+    dma = pltpu.SemaphoreType.DMA
+    bf16, f32 = jnp.bfloat16, jnp.float32
+    anywhere = pl.BlockSpec(memory_space=pl.ANY)
+    vmem = pl.BlockSpec(memory_space=pltpu.VMEM)
+    return pl.pallas_call(
+        functools.partial(expert_kernel, n, tp, cap),
+        out_shape=jax.ShapeDtypeStruct((rows, width), bf16),
+        in_specs=[anywhere, anywhere, vmem, anywhere, anywhere, anywhere],
+        out_specs=vmem,
+        scratch_shapes=[
+            pltpu.VMEM((n, rows, width), bf16),
+            pltpu.VMEM((n,) + table.shape, f32),
+            pltpu.VMEM((2, slots, width), bf16),
+            pltpu.VMEM((n, slots, width), bf16),
+            pltpu.VMEM((n, slots, width), bf16),
+            pltpu.VMEM((n + 1, rows, width), bf16),
+            pltpu.VMEM((rows, width), f32),
+            pltpu.VMEM((width, hidden_width), bf16),
+            pltpu.VMEM((width, hidden_width), bf16),
+            pltpu.VMEM((hidden_width, width), bf16),
+            pltpu.VMEM((slots, hidden_width), bf16),
+            dma((2,)),
+            dma((3,)),
+            dma((2, n)),
+            dma((n,)),
+            dma((2, n)),
+            dma((n,)),
+            dma((n,)),
+            dma((n,)),
+            dma((n,)),
+            dma((n,)),
+            dma((n, CHUNKS)),
+            dma((n + 1, CHUNKS)),
+        ],
+        compiler_params=pltpu.CompilerParams(
+            collective_id=0, has_side_effects=True, vmem_limit_bytes=67043328
+        ),
+        name="experts",
+    )(expert_in, table, after, gate_weight, up_weight, down_weight)
 
 
 def shards(
@@ -65,33 +390,22 @@
     experts = local_count * members
     top_count = expert_ids.shape[1]
     capacity = 2 * top_count * row_count // experts
-    feature_count = expert_in.shape[1]
+    room = -(-capacity // 16) * 16
     flat_ids = expert_ids.reshape(-1)
     onehot = (flat_ids[:, None] == jnp.arange(experts, dtype=jnp.int32)[None, :]).astype(jnp.int32)
     earlier = jnp.sum((jnp.cumsum(onehot, axis=0) - onehot) * onehot, axis=1)
-    target = flat_ids * capacity + earlier
-    source_rows = jnp.repeat(expert_in, top_count, axis=0)
-    outbox = (
-        jnp.zeros((experts * capacity, feature_count), jnp.bfloat16).at[target].set(source_rows)
-    )
-    outbox = outbox.reshape(experts, capacity, feature_count)
-    arrived = lax.all_to_all(outbox, ("sp", "tp"), split_axis=0, concat_axis=0, tiled=True)
-    slot_count = arrived.shape[1]
-    grouped = arrived.reshape(members, local_count, slot_count, feature_count)
-    gate_part = jnp.einsum(
-        "secd,edf->secf", grouped, gate_weight, preferred_element_type=jnp.float32
-    )
-    up_part = jnp.einsum("secd,edf->secf", grouped, up_weight, preferred_element_type=jnp.float32)
-    hidden = (jax.nn.silu(gate_part) * up_part).astype(jnp.bfloat16)
-    answer = jnp.einsum(
-        "secf,efd->secd", hidden, down_weight, preferred_element_type=jnp.float32
-    ).astype(jnp.bfloat16)
-    answer = answer.reshape(members * local_count, slot_count, feature_count)
-    returned = lax.all_to_all(answer, ("sp", "tp"), split_axis=0, concat_axis=0, tiled=True)
-    picked = returned.reshape(experts * capacity, feature_count)[target].astype(jnp.float32)
-    picked = picked.reshape(row_count, top_count, feature_count)
-    routed = jnp.sum(expert_weights[:, :, None] * picked, axis=1)
-    return (after_wide + routed).astype(jnp.bfloat16)
+    target = (flat_ids * room + earlier).reshape(row_count, top_count)
+    table = jnp.concatenate(
+        [
+            target.astype(jnp.float32).T,
+            expert_weights.T,
+            jnp.zeros((8 - 2 * top_count, row_count), jnp.float32),
+        ],
+        axis=0,
+    )
+    return experts_and_back(
+        expert_in, table, after_wide.astype(jnp.bfloat16), gate_weight, up_weight, down_weight, room
+    )
 
 
 def solution(mesh):

time: 200 us -> 159 us (0.80)
  the two profiles are of different devices: /device:TPU:11 before, /device:TPU:0 now
where the time goes in v1:
time: 159 us
  Pallas kernels  96.1 us (60%)
  waiting for transfers between devices  15.2 us (10%)
  between operations  13.5 us (8%)
  starting transfers between devices  9.66 us (6%)
  other arithmetic  7.65 us (5%)
  blocking collectives  7.13 us (4%)
  local copies, waits for them, and re-layouts  6.41 us (4%)
  matrix products  3.03 us (2%)
    pallas_call x1, Pallas kernels, experts_and_back(): pl.pallas_call(functools.partial(expert_kernel, n, tp, cap), out_shape=ja...  96.1 us
    all_to_all x1, waiting for transfers between devices, shards(): lax.all_to_all(activated, 'tp', split_axis=0, concat_axis=1, tiled=True)  8.53 us
    psum x1, blocking collectives, shards(): lax.psum((jnp.sum(mixed_rows, axis=1), jnp.sum(mixed_rows * mixed_rows, a...  7.13 us
    all_gather x1, waiting for transfers between devices, shards(): lax.all_gather(point_weight, 'tp', axis=0, tiled=True)  5.99 us
    ppermute x1, starting transfers between devices, with_halo(): lax.ppermute(lax.slice_in_dim(block, block.shape[dim] - width, None, axis...  4.96 us
    unnamed x12, local copies, waits for them, and re-layouts  3.47 us
    all_to_all x1, starting transfers between devices, shards(): lax.all_to_all(activated, 'tp', split_axis=0, concat_axis=1, tiled=True)  3.41 us
  transfers between devices with their start and end apart: 4, of which 2 were waited for; matrix products, arithmetic and copies ran while one was open for 7% of the time, Pallas kernels for 0%

profile of v1, /device:TPU:0, one launch (start us, length us, event | category | flops | bytes accessed | tf_op | source)
XLA Modules:
  0.0 158.7 jit_solution(2531982375528783561)
XLA Ops:
  6.5 0.7 all-gather.2.cloned.1.call-update
  7.3 1.2 multiply_convert_fusion.1
  8.5 5.0 %collective-permute-start = (bf16[15,256]{1,0:T(8,128)(2,1)S(1)}, bf16[15,256]{1,0:T(8,128)(2,1)S(1)}, u32[]{:S(2)}, u32[]{:S(2)}) collective-permute-start(bf16[15,256]{1,0:T(8,128)(2,1)S(1)} %get-tuple-element.10), channel_id=1, source_target_pairs={{0,4},{4,8},{8,12},{1,5},{5,9},{9,13},{2,6},{6,10},{10,14},{3,7},{... | collective-permute-start | bytes 23048 | tf_op jit(solution)/shard_map/ppermute | solution.py:16
  13.4 1.3 collective-permute-start.1
  14.7 0.8 copy.18
  15.8 0.6 reduce-window.6
  16.4 0.2 slice_reduce_fusion
  16.7 0.1 reduce_sum.42
  16.9 1.0 fusion.42
  17.9 1.0 fusion.41
  18.9 0.7 convert_bitcast_fusion
  19.8 2.4 %fusion.38 = (f32[512]{0:T(512)S(1)}, f32[512]{0:T(512)S(1)}, f32[512,256]{1,0:T(8,128)S(1)}) fusion(f32[542,256]{1,0:T(8,128)S(1)} %maximum_convert_fusion, f32[256]{0:T(256)S(1)} %bitcast.70, f32[256]{0:T(256)S(1)} %bitcast.71, f32[256]{0:T(256)S(1)} %bitcast.73, f32[256]{0:T(256)S(1)} %bitcast.74, f32[256]{0:T(256)S(1)} %bitcast.75, f32[256]{0:T(256)S(1)} %bitcast.76, ...), kind=kLoop, calls=%fused_computation.86 | loop fusion | flops 8387584 | bytes 16813056 | tf_op jit(solution)/shard_map/reduce_sum | solution.py:371
  22.2 7.1 %all-reduce = (f32[512]{0:T(512)S(1)}, f32[512]{0:T(512)S(1)}) all-reduce(f32[512]{0:T(512)S(1)} %get-tuple-element.6, f32[512]{0:T(512)S(1)} %get-tuple-element.5), channel_id=1, replica_groups=mesh['grp'=2,'sp'=4,'tp'=4] {'tp'}, use_global_device_ids=true, to_apply=%region_3.0 | all-reduce | flops 1024 | bytes 8192 | tf_op jit(solution)/shard_map/psum | solution.py:370
  29.4 1.0 multiply_convert_fusion
  30.3 3.4 %all-to-all-start = ((bf16[4,128,256]{2,1,0:T(8,128)(2,1)}), bf16[4,128,256]{2,1,0:T(8,128)(2,1)S(1)}, u32[]{:S(2)}, u32[]{:S(2)}) async-start(bf16[4,128,256]{2,1,0:T(8,128)(2,1)} %bitcast.31), calls=%async_computation | async-start | bytes 524288 | tf_op jit(solution)/shard_map/all_to_all | solution.py:379
  33.7 0.7 maximum_maximum_fusion.tab_hbm
  34.4 8.5 %all-to-all-done = bf16[4,128,256]{2,1,0:T(8,128)(2,1)S(1)} async-done(((bf16[4,128,256]{2,1,0:T(8,128)(2,1)}), bf16[4,128,256]{2,1,0:T(8,128)(2,1)S(1)}, u32[]{:S(2)}, u32[]{:S(2)}) %all-to-all-start) | async-done | bytes 262176 | tf_op jit(solution)/shard_map/all_to_all | solution.py:379
  42.9 0.2 copy.17
  43.1 6.0 %all-gather.2.cloned.1.call-done = bf16[1024,2048]{1,0:T(8,128)(2,1)} async-done(((bf16[256,2048]{1,0:T(8,128)(2,1)}), bf16[1024,2048]{1,0:T(8,128)(2,1)}) %all-gather.2.cloned.1.call-update) | async-done | bytes 4194320 | tf_op jit(solution)/shard_map/all_gather | solution.py:382
  49.1 3.0 %fusion.1 = (f32[128]{0:T(128)S(1)}, bf16[128,2048]{1,0:T(8,128)(2,1)S(1)}) fusion(bf16[128,1024]{0,1:T(8,128)(2,1)S(1)} %bitcast.58, bf16[1024,2048]{1,0:T(8,128)(2,1)} %all-gather.2.cloned.1.call-done, bf16[128,2048]{1,0:T(8,128)(2,1)S(1)} %copy-done.1), kind=kOutput, calls=%fused_computation.4 | convolution fusion | flops 538443648 | bytes 5505536 | tf_op jit(solution)/shard_map/dot_general | solution.py:380
  52.2 0.8 copy-done
  52.9 1.0 fusion.3.x_hbm
  53.9 96.1 %experts.1 = bf16[128,2048]{1,0:T(8,128)(2,1)} custom-call(bf16[128,2048]{1,0:T(8,128)(2,1)} %fusion.3.x_hbm, f32[8,128]{1,0:T(8,128)} %maximum_maximum_fusion.tab_hbm, bf16[128,2048]{1,0:T(8,128)(2,1)} %copy-done, bf16[1,2048,768]{2,1,0:T(8,128)(2,1)} %wg_hbm.1, bf16[1,2048,768]{2,1,0:T(8,128)(2,1)} %wu_hbm.1, bf16[1,768,2048]{2,1,0:T(8,128)(2,1)} %wd_hbm.1), custom_call_target="tpu_custom_call" | custom-call | tf_op jit(solution)/shard_map/experts/pallas_call | solution.py:308
  150.0 1.9 %copy.25 = bf16[128,2048]{1,0:T(8,128)(2,1)} copy(bf16[128,2048]{1,0:T(8,128)(2,1)} %experts.1) | data formatting | bytes 1048576
  (25 shorter events, 0.7 us)
Async XLA Ops:
  6.5 42.6 %all-gather.2.cloned.1.call-start = ((), (), s32[]{:S(2)}) async-start(), calls=%async_computation.1 | async-start | bytes 5242880 | tf_op jit(solution)/shard_map/all_gather | solution.py:382
  8.5 11.3 %collective-permute-start = (bf16[15,256]{1,0:T(8,128)(2,1)S(1)}, bf16[15,256]{1,0:T(8,128)(2,1)S(1)}, u32[]{:S(2)}, u32[]{:S(2)}) collective-permute-start(bf16[15,256]{1,0:T(8,128)(2,1)S(1)} %get-tuple-element.10), channel_id=1, source_target_pairs={{0,4},{4,8},{8,12},{1,5},{5,9},{9,13},{2,6},{6,10},{10,14},{3,7},{... | collective-permute-start | bytes 23048 | tf_op jit(solution)/shard_map/ppermute | solution.py:16
  13.4 6.3 %collective-permute-start.1 = (bf16[15,256]{1,0:T(8,128)(2,1)S(1)}, bf16[15,256]{1,0:T(8,128)(2,1)S(1)}, u32[]{:S(2)}, u32[]{:S(2)}) collective-permute-start(bf16[15,256]{1,0:T(8,128)(2,1)S(1)} %get-tuple-element.11), channel_id=1, source_target_pairs={{4,0},{8,4},{12,8},{5,1},{9,5},{13,9},{6,2},{10,6},{14,10},{7,3},{... | collective-permute-start | bytes 23048 | tf_op jit(solution)/shard_map/ppermute | solution.py:19
  19.8 9.6 %copy-start.3 = (f32[256]{0:T(256)S(1)}, f32[256]{0:T(256)}, u32[]{:S(2)}) copy-start(f32[256]{0:T(256)} %param.16) | copy-start | bytes 3076
  19.8 13.9 %copy-start.4 = (f32[128,2]{0,1:T(2,128)S(1)}, f32[128,2]{0,1:T(2,128)}, u32[]{:S(2)}) copy-start(f32[128,2]{0,1:T(2,128)} %param.20) | copy-start | bytes 3076
  19.8 29.3 %copy-start.1 = (bf16[128,2048]{1,0:T(8,128)(2,1)S(1)}, bf16[128,2048]{1,0:T(8,128)(2,1)}, u32[]{:S(2)}) copy-start(bf16[128,2048]{1,0:T(8,128)(2,1)} %param.12) | copy-start | bytes 1572868
  22.2 30.7 %copy-start.2 = (f32[2048]{0:T(1024)S(1)}, f32[2048]{0:T(1024)}, u32[]{:S(2)}) copy-start(f32[2048]{0:T(1024)} %param.18) | copy-start | bytes 24580
  30.3 12.6 %all-to-all-start = ((bf16[4,128,256]{2,1,0:T(8,128)(2,1)}), bf16[4,128,256]{2,1,0:T(8,128)(2,1)S(1)}, u32[]{:S(2)}, u32[]{:S(2)}) async-start(bf16[4,128,256]{2,1,0:T(8,128)(2,1)} %bitcast.31), calls=%async_computation | async-start | bytes 524288 | tf_op jit(solution)/shard_map/all_to_all | solution.py:379
  52.1 0.8 copy-start
Sparse Core Ops, SparseCore 0:
  8.9 40.1 all-gather.1

commit v2 on v1

--- a/solution.py
+++ b/solution.py
@@ -129,23 +129,38 @@
         place = lax.broadcasted_iota(jnp.int32, (slots, rows), 0).astype(jnp.float32) + base
         return place == table[0:1, :], place == table[1:2, :], table
 
+    def passes_on(zs):
+        return ((zs <= z) & (z < n - 1)) | ((zs >= z) & (z > 0))
+
+    def arrive(zs):
+        pltpu.make_async_copy(tabs.at[zs], tabs.at[zs], tab_recv.at[zs]).wait()
+        pltpu.make_async_copy(toks.at[zs], toks.at[zs], tok_recv.at[zs]).wait()
+
+    def forward(zs):
+        @pl.when((zs <= z) & (z < n - 1))
+        def _():
+            for copy in token_copies(zs, 1):
+                copy.start()
+
+        @pl.when((zs >= z) & (z > 0))
+        def _():
+            for copy in token_copies(zs, 0):
+                copy.start()
+
+    def hand_on(j):
+        zs = source(j)
+
+        @pl.when((j < n) & passes_on(zs))
+        def _():
+            arrive(zs)
+            forward(zs)
+
     def take(j):
         zs = source(j)
 
-        @pl.when(j > 0)
-        def _():
-            pltpu.make_async_copy(tabs.at[zs], tabs.at[zs], tab_recv.at[zs]).wait()
-            pltpu.make_async_copy(toks.at[zs], toks.at[zs], tok_recv.at[zs]).wait()
-
-        @pl.when((zs <= z) & (z < n - 1))
-        def _():
-            for copy in token_copies(zs, 1):
-                copy.start()
-
-        @pl.when((zs >= z) & (z > 0))
-        def _():
-            for copy in token_copies(zs, 0):
-                copy.start()
+        @pl.when((j > 0) & jnp.logical_not(passes_on(zs)))
+        def _():
+            arrive(zs)
 
         first, second, _ = names(zs)
         pick = jnp.where(first | second, 1.0, 0.0).astype(jnp.bfloat16)
@@ -217,10 +232,20 @@
             for k in range(CHUNKS):
                 sum_copy(zs, k, 1).start()
 
+    forward(z)
+
     def body(j, carry):
         @pl.when(j > 0)
         def _():
             run(j - 1)
+
+        @pl.when(j == 1)
+        def _():
+            hand_on(j)
+
+        @pl.when(j > 0)
+        def _():
+            hand_on(j + 1)
 
         @pl.when(j < n)
         def _():

time: 159 us -> 156 us (0.981)
  Pallas kernels: 96.1 us -> 92.3 us
    pallas_call x1, Pallas kernels: 96.1 us -> 92.3 us  [experts_and_back(): pl.pallas_call(functools.partial(expert_kernel, n, tp, cap), out_shape=ja...]
where the time goes in v2:
time: 156 us; the launch traced here: 155 us
  Pallas kernels  92.3 us (59%)
  waiting for transfers between devices  15.2 us (10%)
  between operations  13.5 us (9%)
  starting transfers between devices  9.66 us (6%)
  other arithmetic  7.65 us (5%)
  blocking collectives  7.13 us (5%)
  local copies, waits for them, and re-layouts  6.41 us (4%)
  matrix products  3.03 us (2%)
    pallas_call x1, Pallas kernels, experts_and_back(): pl.pallas_call(functools.partial(expert_kernel, n, tp, cap), out_shape=ja...  92.3 us
    all_to_all x1, waiting for transfers between devices, shards(): lax.all_to_all(activated, 'tp', split_axis=0, concat_axis=1, tiled=True)  8.53 us
    psum x1, blocking collectives, shards(): lax.psum((jnp.sum(mixed_rows, axis=1), jnp.sum(mixed_rows * mixed_rows, a...  7.13 us
    all_gather x1, waiting for transfers between devices, shards(): lax.all_gather(point_weight, 'tp', axis=0, tiled=True)  5.99 us
    ppermute x1, starting transfers between devices, with_halo(): lax.ppermute(lax.slice_in_dim(block, block.shape[dim] - width, None, axis...  4.96 us
    unnamed x12, local copies, waits for them, and re-layouts  3.47 us
    all_to_all x1, starting transfers between devices, shards(): lax.all_to_all(activated, 'tp', split_axis=0, concat_axis=1, tiled=True)  3.41 us
  transfers between devices with their start and end apart: 4, of which 2 were waited for; matrix products, arithmetic and copies ran while one was open for 7% of the time, Pallas kernels for 0%

profile of v2, /device:TPU:0, one launch (start us, length us, event | category | flops | bytes accessed | tf_op | source)
XLA Modules:
  0.0 155.0 jit_solution(14237716415673146854)
XLA Ops:
  6.5 0.7 all-gather.2.cloned.1.call-update
  7.3 1.2 multiply_convert_fusion.1
  8.5 5.0 %collective-permute-start = (bf16[15,256]{1,0:T(8,128)(2,1)S(1)}, bf16[15,256]{1,0:T(8,128)(2,1)S(1)}, u32[]{:S(2)}, u32[]{:S(2)}) collective-permute-start(bf16[15,256]{1,0:T(8,128)(2,1)S(1)} %get-tuple-element.10), channel_id=1, source_target_pairs={{0,4},{4,8},{8,12},{1,5},{5,9},{9,13},{2,6},{6,10},{10,14},{3,7},{... | collective-permute-start | bytes 23048 | tf_op jit(solution)/shard_map/ppermute | solution.py:16
  13.4 1.3 collective-permute-start.1
  14.7 0.8 copy.18
  15.8 0.6 reduce-window.6
  16.4 0.2 slice_reduce_fusion
  16.7 0.1 reduce_sum.42
  16.9 1.0 fusion.42
  17.9 1.0 fusion.41
  18.9 0.7 convert_bitcast_fusion
  19.8 2.4 %fusion.38 = (f32[512]{0:T(512)S(1)}, f32[512]{0:T(512)S(1)}, f32[512,256]{1,0:T(8,128)S(1)}) fusion(f32[542,256]{1,0:T(8,128)S(1)} %maximum_convert_fusion, f32[256]{0:T(256)S(1)} %bitcast.70, f32[256]{0:T(256)S(1)} %bitcast.71, f32[256]{0:T(256)S(1)} %bitcast.73, f32[256]{0:T(256)S(1)} %bitcast.74, f32[256]{0:T(256)S(1)} %bitcast.75, f32[256]{0:T(256)S(1)} %bitcast.76, ...), kind=kLoop, calls=%fused_computation.86 | loop fusion | flops 8387584 | bytes 16813056 | tf_op jit(solution)/shard_map/reduce_sum | solution.py:396
  22.2 7.1 %all-reduce = (f32[512]{0:T(512)S(1)}, f32[512]{0:T(512)S(1)}) all-reduce(f32[512]{0:T(512)S(1)} %get-tuple-element.6, f32[512]{0:T(512)S(1)} %get-tuple-element.5), channel_id=1, replica_groups=mesh['grp'=2,'sp'=4,'tp'=4] {'tp'}, use_global_device_ids=true, to_apply=%region_3.0 | all-reduce | flops 1024 | bytes 8192 | tf_op jit(solution)/shard_map/psum | solution.py:395
  29.4 1.0 multiply_convert_fusion
  30.3 3.4 %all-to-all-start = ((bf16[4,128,256]{2,1,0:T(8,128)(2,1)}), bf16[4,128,256]{2,1,0:T(8,128)(2,1)S(1)}, u32[]{:S(2)}, u32[]{:S(2)}) async-start(bf16[4,128,256]{2,1,0:T(8,128)(2,1)} %bitcast.31), calls=%async_computation | async-start | bytes 524288 | tf_op jit(solution)/shard_map/all_to_all | solution.py:404
  33.7 0.7 maximum_maximum_fusion.tab_hbm
  34.4 8.5 %all-to-all-done = bf16[4,128,256]{2,1,0:T(8,128)(2,1)S(1)} async-done(((bf16[4,128,256]{2,1,0:T(8,128)(2,1)}), bf16[4,128,256]{2,1,0:T(8,128)(2,1)S(1)}, u32[]{:S(2)}, u32[]{:S(2)}) %all-to-all-start) | async-done | bytes 262176 | tf_op jit(solution)/shard_map/all_to_all | solution.py:404
  42.9 0.2 copy.17
  43.1 6.0 %all-gather.2.cloned.1.call-done = bf16[1024,2048]{1,0:T(8,128)(2,1)} async-done(((bf16[256,2048]{1,0:T(8,128)(2,1)}), bf16[1024,2048]{1,0:T(8,128)(2,1)}) %all-gather.2.cloned.1.call-update) | async-done | bytes 4194320 | tf_op jit(solution)/shard_map/all_gather | solution.py:407
  49.1 3.0 %fusion.1 = (f32[128]{0:T(128)S(1)}, bf16[128,2048]{1,0:T(8,128)(2,1)S(1)}) fusion(bf16[128,1024]{0,1:T(8,128)(2,1)S(1)} %bitcast.58, bf16[1024,2048]{1,0:T(8,128)(2,1)} %all-gather.2.cloned.1.call-done, bf16[128,2048]{1,0:T(8,128)(2,1)S(1)} %copy-done.1), kind=kOutput, calls=%fused_computation.4 | convolution fusion | flops 538443648 | bytes 5505536 | tf_op jit(solution)/shard_map/dot_general | solution.py:405
  52.2 0.8 copy-done
  52.9 1.0 fusion.3.x_hbm
  53.9 92.3 %experts.1 = bf16[128,2048]{1,0:T(8,128)(2,1)} custom-call(bf16[128,2048]{1,0:T(8,128)(2,1)} %fusion.3.x_hbm, f32[8,128]{1,0:T(8,128)} %maximum_maximum_fusion.tab_hbm, bf16[128,2048]{1,0:T(8,128)(2,1)} %copy-done, bf16[1,2048,768]{2,1,0:T(8,128)(2,1)} %wg_hbm.1, bf16[1,2048,768]{2,1,0:T(8,128)(2,1)} %wu_hbm.1, bf16[1,768,2048]{2,1,0:T(8,128)(2,1)} %wd_hbm.1), custom_call_target="tpu_custom_call" | custom-call | tf_op jit(solution)/shard_map/experts/pallas_call | solution.py:333
  146.2 1.9 %copy.25 = bf16[128,2048]{1,0:T(8,128)(2,1)} copy(bf16[128,2048]{1,0:T(8,128)(2,1)} %experts.1) | data formatting | bytes 1048576
  (25 shorter events, 0.7 us)
Async XLA Ops:
  6.5 42.6 %all-gather.2.cloned.1.call-start = ((), (), s32[]{:S(2)}) async-start(), calls=%async_computation.1 | async-start | bytes 5242880 | tf_op jit(solution)/shard_map/all_gather | solution.py:407
  8.5 11.3 %collective-permute-start = (bf16[15,256]{1,0:T(8,128)(2,1)S(1)}, bf16[15,256]{1,0:T(8,128)(2,1)S(1)}, u32[]{:S(2)}, u32[]{:S(2)}) collective-permute-start(bf16[15,256]{1,0:T(8,128)(2,1)S(1)} %get-tuple-element.10), channel_id=1, source_target_pairs={{0,4},{4,8},{8,12},{1,5},{5,9},{9,13},{2,6},{6,10},{10,14},{3,7},{... | collective-permute-start | bytes 23048 | tf_op jit(solution)/shard_map/ppermute | solution.py:16
  13.4 6.3 %collective-permute-start.1 = (bf16[15,256]{1,0:T(8,128)(2,1)S(1)}, bf16[15,256]{1,0:T(8,128)(2,1)S(1)}, u32[]{:S(2)}, u32[]{:S(2)}) collective-permute-start(bf16[15,256]{1,0:T(8,128)(2,1)S(1)} %get-tuple-element.11), channel_id=1, source_target_pairs={{4,0},{8,4},{12,8},{5,1},{9,5},{13,9},{6,2},{10,6},{14,10},{7,3},{... | collective-permute-start | bytes 23048 | tf_op jit(solution)/shard_map/ppermute | solution.py:19
  19.8 9.6 %copy-start.3 = (f32[256]{0:T(256)S(1)}, f32[256]{0:T(256)}, u32[]{:S(2)}) copy-start(f32[256]{0:T(256)} %param.16) | copy-start | bytes 3076
  19.8 13.9 %copy-start.4 = (f32[128,2]{0,1:T(2,128)S(1)}, f32[128,2]{0,1:T(2,128)}, u32[]{:S(2)}) copy-start(f32[128,2]{0,1:T(2,128)} %param.20) | copy-start | bytes 3076
  19.8 29.3 %copy-start.1 = (bf16[128,2048]{1,0:T(8,128)(2,1)S(1)}, bf16[128,2048]{1,0:T(8,128)(2,1)}, u32[]{:S(2)}) copy-start(bf16[128,2048]{1,0:T(8,128)(2,1)} %param.12) | copy-start | bytes 1572868
  22.2 30.7 %copy-start.2 = (f32[2048]{0:T(1024)S(1)}, f32[2048]{0:T(1024)}, u32[]{:S(2)}) copy-start(f32[2048]{0:T(1024)} %param.18) | copy-start | bytes 24580
  30.3 12.6 %all-to-all-start = ((bf16[4,128,256]{2,1,0:T(8,128)(2,1)}), bf16[4,128,256]{2,1,0:T(8,128)(2,1)S(1)}, u32[]{:S(2)}, u32[]{:S(2)}) async-start(bf16[4,128,256]{2,1,0:T(8,128)(2,1)} %bitcast.31), calls=%async_computation | async-start | bytes 524288 | tf_op jit(solution)/shard_map/all_to_all | solution.py:404
  52.1 0.8 copy-start
Sparse Core Ops, SparseCore 0:
  8.9 40.1 all-gather.1

commit v3 on v2

--- a/solution.py
+++ b/solution.py
@@ -6,19 +6,6 @@
 from jax.experimental import pallas as pl
 from jax.experimental.pallas import tpu as pltpu
 from jax.sharding import PartitionSpec as P
-
-
-def with_halo(block, sides, width):
-    for axis, dim in sides:
-        count = lax.axis_size(axis)
-        forward = [(i, i + 1) for i in range(count - 1)]
-        backward = [(target, source) for source, target in forward]
-        low = lax.ppermute(
-            lax.slice_in_dim(block, block.shape[dim] - width, None, axis=dim), axis, forward
-        )
-        high = lax.ppermute(lax.slice_in_dim(block, 0, width, axis=dim), axis, backward)
-        block = jnp.concatenate([low, block, high], axis=dim)
-    return block
 
 
 MESH = pl.DeviceIdType.MESH
@@ -367,6 +354,265 @@
     )(expert_in, table, after, gate_weight, up_weight, down_weight)
 
 
+def branch_kernel(
+    n, tp, taps_count, value_ref, gate_ref, taps_ref, weight_ref, latent_ref, gain_ref,
+    after_ref, in_ref,
+    gated, win, low, high, taps, wide, mixed, act, weights, total,
+    win_send, win_recv, halo_send, halo_recv, tap_send, tap_recv, w_send, w_pass, w_recv,
+):
+    z = lax.axis_index("sp")
+    t = lax.axis_index("tp")
+    block, chans = value_ref.shape
+    rows, width = latent_ref.shape
+    edge = low.shape[1]
+    half = taps_count // 2
+    view = rows + 2 * edge
+    mate = t + 1 - 2 * lax.rem(t, 2)
+    halves = chans // 2
+
+    barrier = pltpu.get_barrier_semaphore()
+    for p in range(tp):
+        other = lax.rem(t + p, tp)
+        if p:
+            pl.semaphore_signal(barrier, inc=1, device_id={"tp": other}, device_id_type=MESH)
+
+        @pl.when(z > 0)
+        def _():
+            pl.semaphore_signal(
+                barrier, inc=1, device_id={"sp": z - 1, "tp": other}, device_id_type=MESH
+            )
+
+        @pl.when(z < n - 1)
+        def _():
+            pl.semaphore_signal(
+                barrier, inc=1, device_id={"sp": z + 1, "tp": other}, device_id_type=MESH
+            )
+
+    gated[pl.ds(0, edge)] = jnp.zeros((edge, chans), jnp.bfloat16)
+    gated[pl.ds(edge + block, edge)] = jnp.zeros((edge, chans), jnp.bfloat16)
+    step = 64
+    for r in range(0, block, step):
+        value = value_ref[pl.ds(r, step)].astype(jnp.float32)
+        gate = gate_ref[pl.ds(r, step)].astype(jnp.float32)
+        gated[pl.ds(edge + r, step)] = (value * jax.nn.sigmoid(gate)).astype(jnp.bfloat16)
+
+    peers = tp - 1 + tp * ((z > 0).astype(jnp.int32) + (z < n - 1).astype(jnp.int32))
+    pl.semaphore_wait(barrier, peers)
+
+    def span(index):
+        return pl.ds(pl.multiple_of(index * rows, 16), view)
+
+    def win_copy(p):
+        other = lax.rem(t + p, tp)
+        return pltpu.make_async_remote_copy(
+            src_ref=gated.at[span(other)], dst_ref=win.at[t],
+            send_sem=win_send.at[p], recv_sem=win_recv.at[t],
+            device_id={"tp": other}, device_id_type=MESH,
+        )
+
+    def tap_copy(p):
+        other = lax.rem(t + p, tp)
+        return pltpu.make_async_remote_copy(
+            src_ref=taps_ref, dst_ref=taps.at[t],
+            send_sem=tap_send.at[p], recv_sem=tap_recv.at[t],
+            device_id={"tp": other}, device_id_type=MESH,
+        )
+
+    def halo_copy(up):
+        start = block if up else edge
+        place = low if up else high
+        return pltpu.make_async_remote_copy(
+            src_ref=gated.at[pl.ds(start, edge)], dst_ref=place.at[t],
+            send_sem=halo_send.at[up], recv_sem=halo_recv.at[up, t],
+            device_id={"sp": z + 1 if up else z - 1, "tp": jnp.int32(0 if up else tp - 1)},
+            device_id_type=MESH,
+        )
+
+    @pl.when(z < n - 1)
+    def _():
+        halo_copy(1).start()
+
+    @pl.when(z > 0)
+    def _():
+        halo_copy(0).start()
+
+    for p in range(1, tp):
+        win_copy(p).start()
+        tap_copy(p).start()
+
+    def weight_copy(source, part, target, send_sem, first):
+        spot = pl.ds(part * halves, halves)
+        return pltpu.make_async_remote_copy(
+            src_ref=weight_ref.at[spot] if first else weights.at[source, spot],
+            dst_ref=weights.at[source, spot],
+            send_sem=send_sem, recv_sem=w_recv.at[source, part],
+            device_id={"tp": target}, device_id_type=MESH,
+        )
+
+    def own_weights():
+        copies = []
+        for part in range(2):
+            for q in range(1, tp // 2):
+                copies.append(
+                    weight_copy(t, part, lax.rem(t + 2 * q, tp), w_send.at[q, part], True)
+                )
+            copies.append(weight_copy(t, part, mate, w_send.at[0, part], True))
+        return copies
+
+    for copy in own_weights():
+        copy.start()
+
+    win[t] = gated[span(t)]
+    taps[t] = taps_ref[...]
+    weights[t] = weight_ref[...]
+
+    for p in range(1, tp):
+        other = lax.rem(t + p, tp)
+        pltpu.make_async_copy(win.at[other], win.at[other], win_recv.at[other]).wait()
+        pltpu.make_async_copy(taps.at[other], taps.at[other], tap_recv.at[other]).wait()
+
+    @pl.when((t == 0) & (z > 0))
+    def _():
+        for s in range(tp):
+            pltpu.make_async_copy(low.at[s], low.at[s], halo_recv.at[1, s]).wait()
+            win[s, pl.ds(0, edge)] = low[s]
+
+    @pl.when((t == tp - 1) & (z < n - 1))
+    def _():
+        for s in range(tp):
+            pltpu.make_async_copy(high.at[s], high.at[s], halo_recv.at[0, s]).wait()
+            win[s, pl.ds(edge + rows, edge)] = high[s]
+
+    def convolve(s, carry):
+        first, second = carry
+        wide[...] = win[s].astype(jnp.float32)
+        tile = 64
+        sums, squares = [], []
+        for r in range(0, rows, tile):
+            value = jnp.zeros((tile, chans), jnp.float32)
+            for i in range(taps_count):
+                value = value + taps[s, pl.ds(i, 1)] * wide[pl.ds(edge - half + i + r, tile)]
+            mixed[s, pl.ds(r, tile)] = value
+            sums.append(jnp.sum(value, axis=1, keepdims=True))
+            squares.append(jnp.sum(value * value, axis=1, keepdims=True))
+        return first + jnp.concatenate(sums, axis=0), second + jnp.concatenate(squares, axis=0)
+
+    zero = jnp.zeros((rows, 1), jnp.float32)
+    sums, squares = lax.fori_loop(0, tp, convolve, (zero, zero))
+    center = sums / (chans * tp)
+    spread = squares / (chans * tp) - center * center
+    scale = lax.rsqrt(spread + 0.05)
+
+    def activate(s, carry):
+        value = (mixed[s] - center) * scale * taps[s, pl.ds(taps_count, 1)]
+        act[s] = jax.nn.silu(value).astype(jnp.bfloat16)
+        return carry
+
+    lax.fori_loop(0, tp, activate, 0)
+
+    def multiply(source):
+        for c in range(0, width, 512):
+            spot = pl.ds(c, 512)
+            total[:, spot] += jnp.dot(
+                act[source], weights[source, :, spot], preferred_element_type=jnp.float32
+            )
+
+    def landed(source):
+        for part in range(2):
+            spot = weights.at[source, pl.ds(part * halves, halves)]
+            pltpu.make_async_copy(spot, spot, w_recv.at[source, part]).wait()
+
+    total[...] = latent_ref[...].astype(jnp.float32)
+    multiply(t)
+    landed(mate)
+    multiply(mate)
+
+    def passing(q, part):
+        source = lax.rem(t + 2 * q, tp)
+        return weight_copy(source, part, mate, w_pass.at[q, part], False)
+
+    for q in range(1, tp // 2):
+        source = lax.rem(t + 2 * q, tp)
+        for part in range(2):
+            spot = weights.at[source, pl.ds(part * halves, halves)]
+            pltpu.make_async_copy(spot, spot, w_recv.at[source, part]).wait()
+            passing(q, part).start()
+        multiply(source)
+    for q in range(1, tp // 2):
+        source = lax.rem(mate + 2 * q, tp)
+        landed(source)
+        multiply(source)
+
+    for r in range(0, rows, 32):
+        spot = pl.ds(r, 32)
+        after = total[spot].astype(jnp.bfloat16)
+        after_ref[spot] = after
+        after = after.astype(jnp.float32)
+        norm = lax.rsqrt(jnp.mean(after * after, axis=1, keepdims=True) + 0.01)
+        in_ref[spot] = (after * norm * gain_ref[...]).astype(jnp.bfloat16)
+
+    for p in range(1, tp):
+        win_copy(p).wait_send()
+        tap_copy(p).wait_send()
+    for copy in own_weights():
+        copy.wait_send()
+    for q in range(1, tp // 2):
+        for part in range(2):
+            passing(q, part).wait_send()
+
+    @pl.when(z < n - 1)
+    def _():
+        halo_copy(1).wait_send()
+
+    @pl.when(z > 0)
+    def _():
+        halo_copy(0).wait_send()
+
+
+def branch_and_norm(value, gate, conv_taps, conv_gain, point_weight, latents, channel_gain):
+    n, tp = lax.axis_size("sp"), lax.axis_size("tp")
+    block, chans = value.shape
+    rows, width = latents.shape
+    taps_count = conv_taps.shape[0]
+    edge = -(-(taps_count // 2) // 16) * 16
+    table = jnp.concatenate([conv_taps, conv_gain[None, :]], axis=0)
+    table = jnp.pad(table, ((0, -table.shape[0] % 8), (0, 0)))
+    dma = pltpu.SemaphoreType.DMA
+    bf16, f32 = jnp.bfloat16, jnp.float32
+    vmem = pl.BlockSpec(memory_space=pltpu.VMEM)
+    return pl.pallas_call(
+        functools.partial(branch_kernel, n, tp, taps_count),
+        out_shape=[jax.ShapeDtypeStruct((rows, width), bf16)] * 2,
+        in_specs=[vmem] * 6,
+        out_specs=[vmem] * 2,
+        scratch_shapes=[
+            pltpu.VMEM((block + 2 * edge, chans), bf16),
+            pltpu.VMEM((tp, rows + 2 * edge, chans), bf16),
+            pltpu.VMEM((tp, edge, chans), bf16),
+            pltpu.VMEM((tp, edge, chans), bf16),
+            pltpu.VMEM((tp,) + table.shape, f32),
+            pltpu.VMEM((rows + 2 * edge, chans), f32),
+            pltpu.VMEM((tp, rows, chans), f32),
+            pltpu.VMEM((tp, rows, chans), bf16),
+            pltpu.VMEM((tp, chans, width), bf16),
+            pltpu.VMEM((rows, width), f32),
+            dma((tp,)),
+            dma((tp,)),
+            dma((2,)),
+            dma((2, tp)),
+            dma((tp,)),
+            dma((tp,)),
+            dma((tp // 2, 2)),
+            dma((tp // 2, 2)),
+            dma((tp, 2)),
+        ],
+        compiler_params=pltpu.CompilerParams(
+            collective_id=1, has_side_effects=True, vmem_limit_bytes=48 * 2**20
+        ),
+        name="branch",
+    )(value, gate, table, point_weight, latents, channel_gain[None, :])
+
+
 def shards(
     latents,
     conv_value,
@@ -381,35 +627,10 @@
     up_weight,
     down_weight,
 ):
-    gated_value = (
-        conv_value.astype(jnp.float32) * jax.nn.sigmoid(conv_gate.astype(jnp.float32))
-    ).astype(jnp.bfloat16)
-    tap_count = conv_taps.shape[0]
-    half_span = tap_count // 2
-    block_rows = gated_value.shape[0]
-    padded = with_halo(gated_value, (("sp", 0),), half_span).astype(jnp.float32)
-    mixed_rows = jnp.zeros(gated_value.shape, jnp.float32)
-    for offset in range(tap_count):
-        mixed_rows = mixed_rows + conv_taps[offset][None, :] * padded[offset : offset + block_rows]
-    width_all = conv_value.shape[1] * lax.axis_size("tp")
-    sum_values, squares = lax.psum(
-        (jnp.sum(mixed_rows, axis=1), jnp.sum(mixed_rows * mixed_rows, axis=1)), "tp"
-    )
-    center = (sum_values / width_all)[:, None]
-    spread = (squares / width_all)[:, None] - center * center
-    activated = jax.nn.silu((mixed_rows - center) * lax.rsqrt(spread + 0.05) * conv_gain).astype(
-        jnp.bfloat16
+    after, expert_in = branch_and_norm(
+        conv_value, conv_gate, conv_taps, conv_gain, point_weight, latents, channel_gain
     )
     row_count = latents.shape[0]
-    by_token = lax.all_to_all(activated, "tp", split_axis=0, concat_axis=1, tiled=True)
-    branch = jnp.dot(
-        by_token,
-        lax.all_gather(point_weight, "tp", axis=0, tiled=True),
-        preferred_element_type=jnp.float32,
-    )
-    after_wide = (latents.astype(jnp.float32) + branch).astype(jnp.bfloat16).astype(jnp.float32)
-    scale_rows = lax.rsqrt(jnp.mean(after_wide * after_wide, axis=1, keepdims=True) + 0.01)
-    expert_in = (after_wide * scale_rows * channel_gain).astype(jnp.bfloat16)
     local_count = gate_weight.shape[0]
     members = lax.axis_size(("sp", "tp"))
     experts = local_count * members
@@ -429,7 +650,7 @@
         axis=0,
     )
     return experts_and_back(
-        expert_in, table, after_wide.astype(jnp.bfloat16), gate_weight, up_weight, down_weight, room
+        expert_in, table, after, gate_weight, up_weight, down_weight, room
     )
 
 

time: 156 us -> 141 us (0.904)
  Pallas kernels: 92.3 us -> 127 us
  waiting for transfers between devices: 15.2 us -> 0 us
  between operations: 13.5 us -> 0.06 us
  starting transfers between devices: 9.66 us -> 0 us
  blocking collectives: 7.13 us -> 0 us
  other arithmetic: 7.65 us -> 3.55 us
  local copies, waits for them, and re-layouts: 6.41 us -> 9.85 us
  matrix products: 3.03 us -> 0 us
    pallas_call x0 -> x1, Pallas kernels: none -> 34.8 us  [branch_and_norm(): pl.pallas_call(functools.partial(branch_kernel, n, tp, taps_count), out_s...]
    all_to_all x1 -> x0, waiting for transfers between devices: 8.53 us -> none  [shards(): lax.all_to_all(activated, 'tp', split_axis=0, concat_axis=1, tiled=True)]
    psum x1 -> x0, blocking collectives: 7.13 us -> none  [shards(): lax.psum((jnp.sum(mixed_rows, axis=1), jnp.sum(mixed_rows * mixed_rows, a...]
    ppermute x2 -> x0, starting transfers between devices: 6.25 us -> none  [the longest x1 4.96 us: with_halo(): lax.ppermute(lax.slice_in_dim(block, block.shape[dim] - width, None, axis...]
    all_gather x1 -> x0, waiting for transfers between devices: 5.99 us -> none  [shards(): lax.all_gather(point_weight, 'tp', axis=0, tiled=True)]
    unnamed x12 -> x16, local copies, waits for them, and re-layouts: 3.47 us -> 9.1 us
    all_to_all x1 -> x0, starting transfers between devices: 3.41 us -> none  [shards(): lax.all_to_all(activated, 'tp', split_axis=0, concat_axis=1, tiled=True)]
    convert_element_type x4 -> x0, other arithmetic: 3.18 us -> none  [the longest x1 1.18 us: shards(): gated_value = (conv_value.astype(jnp.float32) * jax.nn.sigmoid(conv_gate....]
  transfers between devices with their start and end apart: 4 -> 0, of which waited for: 2 -> 0; matrix products, arithmetic and copies ran while one was open for 7% -> 0% of each run, Pallas kernels for 0% -> 0%
where the time goes in v3:
time: 141 us; the launch traced here: 140 us
  Pallas kernels  127 us (90%)
  local copies, waits for them, and re-layouts  9.85 us (7%)
  other arithmetic  3.55 us (3%)
    pallas_call x1, Pallas kernels, experts_and_back(): pl.pallas_call(functools.partial(expert_kernel, n, tp, cap), out_shape=ja...  92.1 us
    pallas_call x1, Pallas kernels, branch_and_norm(): pl.pallas_call(functools.partial(branch_kernel, n, tp, taps_count), out_s...  34.8 us
    unnamed x16, local copies, waits for them, and re-layouts  9.1 us

profile of v3, /device:TPU:0, one launch (start us, length us, event | category | flops | bytes accessed | tf_op | source)
XLA Modules:
  0.0 140.4 jit_solution(3659473368286388239)
XLA Ops:
  0.0 0.1 pad.2.clone
  0.1 0.8 pad_maximum_fusion.taps_ref
  0.9 0.8 copy.13
  1.6 0.1 eq.29
  1.8 0.1 eq.25
  1.9 0.6 reduce-window.6
  2.5 0.2 slice_reduce_fusion
  2.8 0.1 fusion.2
  2.9 0.1 reduce_sum.12
  3.0 0.1 copy.16
  3.1 0.7 convert_bitcast_fusion
  3.8 1.3 maximum_maximum_fusion.tab_hbm
  5.1 0.0 copy-start
  5.1 1.2 copy-done
  6.3 1.0 copy-done.3
  7.4 0.9 copy-done.4
  8.3 0.9 copy-done.5
  9.3 0.7 copy-done.6
  10.0 34.8 %branch.1 = (bf16[128,2048]{1,0:T(8,128)(2,1)S(1)}, bf16[128,2048]{1,0:T(8,128)(2,1)S(1)}) custom-call(bf16[512,256]{1,0:T(8,128)(2,1)S(1)} %copy-done.4, bf16[512,256]{1,0:T(8,128)(2,1)S(1)} %copy-done.5, f32[32,256]{1,0:T(8,128)S(1)} %pad_maximum_fusion.taps_ref, bf16[256,2048]{1,0:T(8,128)(2,1)S(1)} %copy-done, bf16[128,2048]{1,0:T(8,128)(2,1)S(1)} %copy-done.3, ...), custom_call_target="tpu_custom_call" | custom-call | tf_op jit(solution)/shard_map/branch/pallas_call | solution.py:583
  44.8 0.0 copy-start.1
  44.8 0.8 copy-done.1
  45.6 0.8 copy-done.2
  46.4 92.1 %experts.1 = bf16[128,2048]{1,0:T(8,128)(2,1)} custom-call(bf16[128,2048]{1,0:T(8,128)(2,1)} %copy-done.2, f32[8,128]{1,0:T(8,128)} %maximum_maximum_fusion.tab_hbm, bf16[128,2048]{1,0:T(8,128)(2,1)} %copy-done.1, bf16[1,2048,768]{2,1,0:T(8,128)(2,1)} %wg_hbm.1, bf16[1,2048,768]{2,1,0:T(8,128)(2,1)} %wu_hbm.1, bf16[1,768,2048]{2,1,0:T(8,128)(2,1)} %wd_hbm.1), custom_call_target="tpu_custom_call" | custom-call | tf_op jit(solution)/shard_map/experts/pallas_call | solution.py:320
  138.5 1.9 %copy.20 = bf16[128,2048]{1,0:T(8,128)(2,1)} copy(bf16[128,2048]{1,0:T(8,128)(2,1)} %experts.1) | data formatting | bytes 1048576
  (9 shorter events, 0.1 us)
Async XLA Ops:
  5.1 1.2 copy-start
  6.3 1.0 copy-start.3
  7.4 0.9 copy-start.4
  8.3 0.9 copy-start.5
  9.3 0.7 copy-start.6
  44.8 0.8 copy-start.1
  45.6 0.8 copy-start.2

commit v4 on v3

--- a/solution.py
+++ b/solution.py
@@ -9,7 +9,7 @@
 
 
 MESH = pl.DeviceIdType.MESH
-CHUNKS = 4
+CHUNKS = 8
 
 
 def expert_kernel(
@@ -355,9 +355,9 @@
 
 
 def branch_kernel(
-    n, tp, taps_count, value_ref, gate_ref, taps_ref, weight_ref, latent_ref, gain_ref,
-    after_ref, in_ref,
-    gated, win, low, high, taps, wide, mixed, act, weights, total,
+    n, tp, taps_count, room, value_hbm, gate_hbm, taps_ref, weight_hbm, latent_hbm, gain_ref,
+    ids_ref, share_ref, after_ref, in_ref, table_ref,
+    value_ref, gate_ref, latent_ref, load_sem, gated, win, low, high, taps, wide, mixed, act, weights, total,
     win_send, win_recv, halo_send, halo_recv, tap_send, tap_recv, w_send, w_pass, w_recv,
 ):
     z = lax.axis_index("sp")
@@ -369,6 +369,19 @@
     view = rows + 2 * edge
     mate = t + 1 - 2 * lax.rem(t, 2)
     halves = chans // 2
+    loads = [
+        pltpu.make_async_copy(a, b, load_sem.at[i])
+        for i, (a, b) in enumerate(
+            (
+                (value_hbm, value_ref),
+                (gate_hbm, gate_ref),
+                (weight_hbm, weights.at[t]),
+                (latent_hbm, latent_ref),
+            )
+        )
+    ]
+    for load in loads:
+        load.start()
 
     barrier = pltpu.get_barrier_semaphore()
     for p in range(tp):
@@ -390,6 +403,8 @@
 
     gated[pl.ds(0, edge)] = jnp.zeros((edge, chans), jnp.bfloat16)
     gated[pl.ds(edge + block, edge)] = jnp.zeros((edge, chans), jnp.bfloat16)
+    loads[0].wait()
+    loads[1].wait()
     step = 64
     for r in range(0, block, step):
         value = value_ref[pl.ds(r, step)].astype(jnp.float32)
@@ -440,10 +455,12 @@
         win_copy(p).start()
         tap_copy(p).start()
 
-    def weight_copy(source, part, target, send_sem, first):
+    loads[2].wait()
+
+    def weight_copy(source, part, target, send_sem):
         spot = pl.ds(part * halves, halves)
         return pltpu.make_async_remote_copy(
-            src_ref=weight_ref.at[spot] if first else weights.at[source, spot],
+            src_ref=weights.at[source, spot],
             dst_ref=weights.at[source, spot],
             send_sem=send_sem, recv_sem=w_recv.at[source, part],
             device_id={"tp": target}, device_id_type=MESH,
@@ -454,9 +471,9 @@
         for part in range(2):
             for q in range(1, tp // 2):
                 copies.append(
-                    weight_copy(t, part, lax.rem(t + 2 * q, tp), w_send.at[q, part], True)
+                    weight_copy(t, part, lax.rem(t + 2 * q, tp), w_send.at[q, part])
                 )
-            copies.append(weight_copy(t, part, mate, w_send.at[0, part], True))
+            copies.append(weight_copy(t, part, mate, w_send.at[0, part]))
         return copies
 
     for copy in own_weights():
@@ -464,7 +481,28 @@
 
     win[t] = gated[span(t)]
     taps[t] = taps_ref[...]
-    weights[t] = weight_ref[...]
+
+    top_count = ids_ref.shape[1]
+    spread_out = [
+        jnp.broadcast_to(ids_ref[:, k : k + 1].astype(jnp.float32), (rows, rows))
+        for k in range(top_count)
+    ]
+    across = [value.T for value in spread_out]
+    down_place = lax.broadcasted_iota(jnp.int32, (rows, rows), 0)
+    across_place = lax.broadcasted_iota(jnp.int32, (rows, rows), 1)
+    table_ref[...] = jnp.zeros_like(table_ref)
+    for k in range(top_count):
+        count = jnp.zeros((1, rows), jnp.float32)
+        for m in range(k + 1):
+            same = spread_out[m] == across[k]
+            if m == k:
+                same = same & (down_place < across_place)
+            count = count + jnp.sum(jnp.where(same, 1.0, 0.0), axis=0, keepdims=True)
+        table_ref[pl.ds(k, 1)] = across[k][0:1] * room + count
+        table_ref[pl.ds(top_count + k, 1)] = jnp.broadcast_to(
+            share_ref[:, k : k + 1], (rows, rows)
+        ).T[0:1]
+
 
     for p in range(1, tp):
         other = lax.rem(t + p, tp)
@@ -522,6 +560,7 @@
             spot = weights.at[source, pl.ds(part * halves, halves)]
             pltpu.make_async_copy(spot, spot, w_recv.at[source, part]).wait()
 
+    loads[3].wait()
     total[...] = latent_ref[...].astype(jnp.float32)
     multiply(t)
     landed(mate)
@@ -529,7 +568,7 @@
 
     def passing(q, part):
         source = lax.rem(t + 2 * q, tp)
-        return weight_copy(source, part, mate, w_pass.at[q, part], False)
+        return weight_copy(source, part, mate, w_pass.at[q, part])
 
     for q in range(1, tp // 2):
         source = lax.rem(t + 2 * q, tp)
@@ -569,7 +608,9 @@
         halo_copy(0).wait_send()
 
 
-def branch_and_norm(value, gate, conv_taps, conv_gain, point_weight, latents, channel_gain):
+def branch_and_norm(
+    value, gate, conv_taps, conv_gain, point_weight, latents, channel_gain, ids, shares, room
+):
     n, tp = lax.axis_size("sp"), lax.axis_size("tp")
     block, chans = value.shape
     rows, width = latents.shape
@@ -579,13 +620,19 @@
     table = jnp.pad(table, ((0, -table.shape[0] % 8), (0, 0)))
     dma = pltpu.SemaphoreType.DMA
     bf16, f32 = jnp.bfloat16, jnp.float32
+    anywhere = pl.BlockSpec(memory_space=pl.ANY)
     vmem = pl.BlockSpec(memory_space=pltpu.VMEM)
     return pl.pallas_call(
-        functools.partial(branch_kernel, n, tp, taps_count),
-        out_shape=[jax.ShapeDtypeStruct((rows, width), bf16)] * 2,
-        in_specs=[vmem] * 6,
-        out_specs=[vmem] * 2,
+        functools.partial(branch_kernel, n, tp, taps_count, room),
+        out_shape=[jax.ShapeDtypeStruct((rows, width), bf16)] * 2
+        + [jax.ShapeDtypeStruct((8, rows), f32)],
+        in_specs=[anywhere, anywhere, vmem, anywhere, anywhere, vmem, vmem, vmem],
+        out_specs=[vmem] * 3,
         scratch_shapes=[
+            pltpu.VMEM((block, chans), bf16),
+            pltpu.VMEM((block, chans), bf16),
+            pltpu.VMEM((rows, width), bf16),
+            dma((4,)),
             pltpu.VMEM((block + 2 * edge, chans), bf16),
             pltpu.VMEM((tp, rows + 2 * edge, chans), bf16),
             pltpu.VMEM((tp, edge, chans), bf16),
@@ -610,7 +657,7 @@
             collective_id=1, has_side_effects=True, vmem_limit_bytes=48 * 2**20
         ),
         name="branch",
-    )(value, gate, table, point_weight, latents, channel_gain[None, :])
+    )(value, gate, table, point_weight, latents, channel_gain[None, :], ids, shares)
 
 
 def shards(
@@ -627,27 +674,13 @@
     up_weight,
     down_weight,
 ):
-    after, expert_in = branch_and_norm(
-        conv_value, conv_gate, conv_taps, conv_gain, point_weight, latents, channel_gain
-    )
-    row_count = latents.shape[0]
-    local_count = gate_weight.shape[0]
-    members = lax.axis_size(("sp", "tp"))
-    experts = local_count * members
-    top_count = expert_ids.shape[1]
+    row_count, top_count = expert_ids.shape
+    experts = gate_weight.shape[0] * lax.axis_size(("sp", "tp"))
     capacity = 2 * top_count * row_count // experts
     room = -(-capacity // 16) * 16
-    flat_ids = expert_ids.reshape(-1)
-    onehot = (flat_ids[:, None] == jnp.arange(experts, dtype=jnp.int32)[None, :]).astype(jnp.int32)
-    earlier = jnp.sum((jnp.cumsum(onehot, axis=0) - onehot) * onehot, axis=1)
-    target = (flat_ids * room + earlier).reshape(row_count, top_count)
-    table = jnp.concatenate(
-        [
-            target.astype(jnp.float32).T,
-            expert_weights.T,
-            jnp.zeros((8 - 2 * top_count, row_count), jnp.float32),
-        ],
-        axis=0,
+    after, expert_in, table = branch_and_norm(
+        conv_value, conv_gate, conv_taps, conv_gain, point_weight, latents, channel_gain,
+        expert_ids, expert_weights, room,
     )
     return experts_and_back(
         expert_in, table, after, gate_weight, up_weight, down_weight, room

time: 141 us -> 138 us (0.979)
  other arithmetic: 3.55 us -> 0.78 us
    unnamed x16 -> x19, local copies, waits for them, and re-layouts: 9.1 us -> 10.5 us
where the time goes in v4:
time: 138 us; the launch traced here: 137 us
  Pallas kernels  126 us (91%)
  local copies, waits for them, and re-layouts  10.5 us (8%)
    pallas_call x1, Pallas kernels, experts_and_back(): pl.pallas_call(functools.partial(expert_kernel, n, tp, cap), out_shape=ja...  90.9 us
    pallas_call x1, Pallas kernels, branch_and_norm(): pl.pallas_call(functools.partial(branch_kernel, n, tp, taps_count, room),...  35.1 us
    unnamed x19, local copies, waits for them, and re-layouts  10.5 us

profile of v4, /device:TPU:0, one launch (start us, length us, event | category | flops | bytes accessed | tf_op | source)
XLA Modules:
  0.0 137.3 jit_solution(3440859396773438181)
XLA Ops:
  0.0 0.8 pad_maximum_fusion.taps_ref
  0.8 0.8 copy.13.ids_ref
  1.6 0.8 copy.14.share_ref
  2.4 0.0 copy-start
  2.4 1.2 copy-done
  3.6 0.0 copy-start.1
  3.6 1.0 copy-done.1
  4.6 0.0 copy-start.4
  4.6 0.9 copy-done.4
  5.6 0.0 copy-start.5
  5.6 0.9 copy-done.5
  6.5 0.0 copy-start.6
  6.5 0.7 copy-done.6
  7.2 35.1 %branch.1 = (bf16[128,2048]{1,0:T(8,128)(2,1)S(1)}, bf16[128,2048]{1,0:T(8,128)(2,1)S(1)}, f32[8,128]{1,0:T(8,128)S(1)}) custom-call(bf16[512,256]{1,0:T(8,128)(2,1)S(1)} %copy-done.4, bf16[512,256]{1,0:T(8,128)(2,1)S(1)} %copy-done.5, f32[32,256]{1,0:T(8,128)S(1)} %pad_maximum_fusion.taps_ref, bf16[256,2048]{1,0:T(8,128)(2,1)S(1)} %copy-done, ...), custom_call_target="tpu_custom_call" | custom-call | tf_op jit(solution)/shard_map/branch/pallas_call | solution.py:625
  42.3 0.0 copy-start.2
  42.3 0.8 copy-done.2
  43.1 0.0 copy-start.3
  43.1 0.8 copy-done.3
  43.9 0.0 copy-start.7
  43.9 0.6 copy-done.7
  44.5 90.9 %experts.1 = bf16[128,2048]{1,0:T(8,128)(2,1)} custom-call(bf16[128,2048]{1,0:T(8,128)(2,1)} %copy-done.3, f32[8,128]{1,0:T(8,128)} %copy-done.7, bf16[128,2048]{1,0:T(8,128)(2,1)} %copy-done.2, bf16[1,2048,768]{2,1,0:T(8,128)(2,1)} %wg_hbm.1, bf16[1,2048,768]{2,1,0:T(8,128)(2,1)} %wu_hbm.1, bf16[1,768,2048]{2,1,0:T(8,128)(2,1)} %wd_hbm.1), custom_call_target="tpu_custom_call" | custom-call | tf_op jit(solution)/shard_map/experts/pallas_call | solution.py:320
  135.4 1.9 %copy.16 = bf16[128,2048]{1,0:T(8,128)(2,1)} copy(bf16[128,2048]{1,0:T(8,128)(2,1)} %experts.1) | data formatting | bytes 1048576
Async XLA Ops:
  2.4 1.2 copy-start
  3.6 1.0 copy-start.1
  4.6 0.9 copy-start.4
  5.6 0.9 copy-start.5
  6.5 0.7 copy-start.6
  42.3 0.8 copy-start.2
  43.1 0.8 copy-start.3
  43.9 0.6 copy-start.7

commit v5 on v4

--- a/solution.py
+++ b/solution.py
@@ -654,7 +654,7 @@
             dma((tp, 2)),
         ],
         compiler_params=pltpu.CompilerParams(
-            collective_id=1, has_side_effects=True, vmem_limit_bytes=48 * 2**20
+            collective_id=1, has_side_effects=True, vmem_limit_bytes=67043328
         ),
         name="branch",
     )(value, gate, table, point_weight, latents, channel_gain[None, :], ids, shares)

time: 138 us -> 134 us (0.971)
  local copies, waits for them, and re-layouts: 10.5 us -> 4.71 us
  Pallas kernels: 126 us -> 128 us
    unnamed x19 -> x3, local copies, waits for them, and re-layouts: 10.5 us -> 4.71 us
    pallas_call x1, Pallas kernels: 35.1 us -> 36.7 us  [branch_and_norm(): pl.pallas_call(functools.partial(branch_kernel, n, tp, taps_count, room),...]
where the time goes in v5:
time: 134 us
  Pallas kernels  128 us (96%)
  local copies, waits for them, and re-layouts  4.71 us (4%)
  other arithmetic  1.39 us (1%)
    pallas_call x1, Pallas kernels, experts_and_back(): pl.pallas_call(functools.partial(expert_kernel, n, tp, cap), out_shape=ja...  91 us
    pallas_call x1, Pallas kernels, branch_and_norm(): pl.pallas_call(functools.partial(branch_kernel, n, tp, taps_count, room),...  36.7 us
    unnamed x3, local copies, waits for them, and re-layouts  4.71 us

profile of v5, /device:TPU:0, one launch (start us, length us, event | category | flops | bytes accessed | tf_op | source)
XLA Modules:
  0.0 133.9 jit_solution(16187107089058798683)
XLA Ops:
  0.0 1.4 %pad_maximum_fusion.taps_ref = f32[32,256]{1,0:T(8,128)} fusion(f32[1,256]{1,0:T(1,128)} %bitcast.3, f32[31,256]{1,0:T(8,128)} %param.15), kind=kLoop, calls=%fused_computation | loop fusion | flops 8192 | bytes 65536 | tf_op jit(solution)/shard_map/concatenate | solution.py:619
  1.4 1.4 %copy.13.ids_ref = s32[128,2]{1,0:T(8,128)} copy(s32[128,2]{0,1:T(2,128)} %param.19) | data formatting | bytes 2048 | tf_op args[7]
  2.8 1.4 %copy.14.share_ref = f32[128,2]{1,0:T(8,128)} copy(f32[128,2]{0,1:T(2,128)} %param.20) | data formatting | bytes 2048 | tf_op args[8]
  4.2 36.7 %branch.1 = (bf16[128,2048]{1,0:T(8,128)(2,1)}, bf16[128,2048]{1,0:T(8,128)(2,1)}, f32[8,128]{1,0:T(8,128)}) custom-call(bf16[512,256]{1,0:T(8,128)(2,1)} %value_hbm.1, bf16[512,256]{1,0:T(8,128)(2,1)} %gate_hbm.1, f32[32,256]{1,0:T(8,128)} %pad_maximum_fusion.taps_ref, bf16[256,2048]{1,0:T(8,128)(2,1)} %weight_hbm.1, bf16[128,2048]{1,0:T(8,128)(2,1)} %latent_hbm.1, ...), custom_call_target="tpu_custom_call" | custom-call | tf_op jit(solution)/shard_map/branch/pallas_call | solution.py:625
  41.0 91.0 %experts.1 = bf16[128,2048]{1,0:T(8,128)(2,1)} custom-call(bf16[128,2048]{1,0:T(8,128)(2,1)} %get-tuple-element.8.x_hbm, f32[8,128]{1,0:T(8,128)} %get-tuple-element.9.tab_hbm, bf16[128,2048]{1,0:T(8,128)(2,1)} %get-tuple-element.10.after_ref, bf16[1,2048,768]{2,1,0:T(8,128)(2,1)} %wg_hbm.1, bf16[1,2048,768]{2,1,0:T(8,128)(2,1)} %wu_hbm.1, ...), custom_call_target="tpu_custom_call" | custom-call | tf_op jit(solution)/shard_map/experts/pallas_call | solution.py:320
  132.0 1.9 %copy.16 = bf16[128,2048]{1,0:T(8,128)(2,1)} copy(bf16[128,2048]{1,0:T(8,128)(2,1)} %experts.1) | data formatting | bytes 1048576
